TPU v7x, 512 devices: a whole 4x4x16 slice. The times are simulated.
512 devices in a mesh: ep: 32 (over z, core), tp: 16 (over y, x).
Axes of the slice: x: 4, y: 4, z: 16, core: 2. Of those that a mesh axis runs over, the one named last changes fastest.
Arguments:
- tokens: bfloat16 [1024, 2048], P('ep', 'tp'), may hold values from -200 to 200
- routing: int32 [1024, 4], P('ep'), may hold values from 0 to 63, all different within a row; in each aligned block of 32 rows (0 to 31, 32 to 63, ...) at most 8 rows name the same one
- gate_weights: float32 [1024, 4], P('ep'), may hold values from 0.05 to 1
- norm_gain: float32 [2048], replicated, may hold values from 0.1 to 1.9
- w_gate: bfloat16 [64, 2048, 2048], P('ep', None, 'tp'), may hold values from -0.33007812 to 0.33007812
- w_up: bfloat16 [64, 2048, 2048], P('ep', None, 'tp'), may hold values from -0.33007812 to 0.33007812
- w_down: bfloat16 [64, 2048, 2048], P('ep', 'tp'), may hold values from -0.026489258 to 0.026489258
Outputs:
- mixed: bfloat16 [1024, 2048], P('ep', 'tp')
Inputs may be any that keep to these rules, and one draw needn't show every extreme that they name: `routing`: each token names 4 different experts. Among the 32 tokens of one index of ep no expert is named more than 8 times, a bound that some block reaches.
All inputs are finite; a program needn't handle non-finite values.
Results may differ from a plain program's by a relative error of at most 0.015.
Values may be sent and summed in bfloat16 or wider, within the bound.
A program may use at most 128 MiB of HBM per device.

v0:
```python
import functools

import jax
import jax.numpy as jnp
from jax import lax
from jax.sharding import Mesh
from jax.sharding import PartitionSpec as P

D = 2048
CAP = 8
TP = ("tp_0", "tp_1")


norm_eps = 1e-06
clamp_limit = 7.0
swish_alpha = 1.702


def one_axis_at_a_time(array, axes):
    return functools.reduce(lax.psum, axes, array)


def sent_to_all(array, axis):
    copies = jnp.broadcast_to(array, (lax.axis_size(axis), *array.shape))
    return lax.all_to_all(copies, axis, split_axis=0, concat_axis=0, tiled=True)


def in_order(pieces, dim):
    pieces = jnp.moveaxis(pieces, 0, dim)
    shape = pieces.shape
    return pieces.reshape(*shape[:dim], shape[dim] * shape[dim + 1], *shape[dim + 2 :])


def gathered_copies(array, axis, dim):
    pieces = sent_to_all(array, axis)
    return in_order(pieces, dim)


def in_blocks(array, dim, length):
    shape = array.shape
    pieces = array.reshape(*shape[:dim], length, shape[dim] // length, *shape[dim + 1 :])
    return jnp.moveaxis(pieces, dim, 0)


def summed_on_arrival(array, axis, dim):
    pieces = in_blocks(array, dim, lax.axis_size(axis))
    arrived = lax.all_to_all(pieces, axis, split_axis=0, concat_axis=0, tiled=True)
    return arrived.astype(jnp.float32).sum(axis=0)


def activate(pre_gate, pre_up):
    clamped = jnp.minimum(pre_gate, clamp_limit)
    upper = jnp.clip(pre_up, -clamp_limit, clamp_limit)
    return (clamped * jax.nn.sigmoid(swish_alpha * clamped) * (upper + 1.0)).astype(jnp.bfloat16)


def per_device(tokens, routing, gate_weights, norm_gain, w_gate, w_up, w_down):
    ep_size = lax.axis_size("ep")
    exp_here = w_gate.shape[0]
    expert_count = exp_here * ep_size
    tok_rows = tokens.shape[0]
    top_count = routing.shape[1]
    col_width = tokens.shape[1]
    chosen = routing.reshape(-1)
    onehot = (chosen[:, None] == jnp.arange(expert_count, dtype=jnp.int32)[None, :]).astype(
        jnp.int32
    )
    slot_rank = jnp.sum(jnp.cumsum(onehot, axis=0) * onehot, axis=1) - 1
    slot_index = (chosen * CAP + slot_rank).reshape(tok_rows, top_count)
    slot_ids = jnp.arange(expert_count * CAP, dtype=jnp.int32)
    matches = slot_ids[:, None, None] == slot_index[None, :, :]
    placing = jnp.sum(matches.astype(jnp.float32), axis=2).astype(jnp.bfloat16)
    wide = tokens.astype(jnp.float32)
    ssq = one_axis_at_a_time(jnp.sum(wide * wide, axis=1), TP)
    gain_cols = lax.dynamic_slice_in_dim(norm_gain, lax.axis_index(TP) * col_width, col_width)
    normed = (wide * lax.rsqrt(ssq / D + norm_eps)[:, None] * gain_cols[None, :]).astype(
        jnp.bfloat16
    )
    outgoing = jnp.dot(placing, normed, preferred_element_type=jnp.float32).astype(jnp.bfloat16)
    outgoing = outgoing.reshape(ep_size, exp_here, CAP, col_width)
    received = lax.all_to_all(outgoing, "ep", split_axis=0, concat_axis=0, tiled=True)
    block_cols = gathered_copies(received, TP, 3)
    gate_part = jnp.einsum("secd,edf->secf", block_cols, w_gate, preferred_element_type=jnp.float32)
    up_part = jnp.einsum("secd,edf->secf", block_cols, w_up, preferred_element_type=jnp.float32)
    hidden = activate(gate_part, up_part)
    partial_value = jnp.einsum("secf,efd->secd", hidden, w_down, preferred_element_type=jnp.float32)
    summed = summed_on_arrival(partial_value.astype(jnp.bfloat16), TP, 3).astype(jnp.bfloat16)
    returned = lax.all_to_all(summed, "ep", split_axis=0, concat_axis=0, tiled=True)
    returned = returned.reshape(expert_count * CAP, col_width).astype(jnp.float32)
    combine = jnp.sum(matches.astype(jnp.float32) * gate_weights[None, :, :], axis=2)
    mixed = jnp.dot(combine.T, returned, precision=lax.Precision.HIGHEST)
    return mixed.astype(jnp.bfloat16)


def solution(mesh):
    split = Mesh(mesh.devices.reshape(mesh.shape["ep"], 4, 4), ("ep", "tp_0", "tp_1"))
    placed = (
        P("ep", TP),
        P("ep", None),
        P("ep", None),
        P(),
        P("ep", None, TP),
        P("ep", None, TP),
        P("ep", TP, None),
    )
    return jax.shard_map(
        per_device, mesh=split, in_specs=placed, out_specs=P("ep", TP), check_vma=False
    )
```

profile of v0, /device:TPU:1, one launch (start us, length us, event | category | flops | bytes accessed | tf_op | source)
XLA Modules:
  0.0 149.6 jit_solution(17330649923930033378)
XLA Ops:
  0.0 0.0 copy-start
  0.0 0.9 fusion.48
  0.9 9.5 %psum.14 = f32[32]{0:T(128)S(1)} all-reduce(f32[32]{0:T(128)S(1)} %fusion.48), channel_id=1, replica_groups=mesh['ep'=32,'tp_0'=4,'tp_1'=4] {'tp_0'}, use_global_device_ids=true, to_apply=%region_5.6 | all-reduce | flops 32 | bytes 256 | tf_op jit(solution)/shard_map/psum | solution.py:20
  10.4 8.5 %psum.15 = f32[32]{0:T(128)S(1)} all-reduce(f32[32]{0:T(128)S(1)} %psum.14), channel_id=1, replica_groups=mesh['ep'=32,'tp_0'=4,'tp_1'=4] {'tp_1'}, use_global_device_ids=true, to_apply=%region_6.7 | all-reduce | flops 32 | bytes 256 | tf_op jit(solution)/shard_map/psum | solution.py:20
  18.9 0.8 copy.53
  19.7 0.1 eq.29
  19.8 0.1 fusion.46
  19.9 0.2 reduce_window_sum.11
  20.0 0.2 select_reduce_fusion.1
  20.2 0.1 sub.7
  20.3 0.1 copy.54
  20.4 0.7 multiply_add_fusion
  21.1 0.8 dynamic_slice.3
  21.9 0.8 convert_reduce_fusion
  22.7 0.9 convolution_convert_fusion.1
  23.6 35.6 %all_to_all.20 = bf16[32,2,8,128]{3,2,1,0:T(8,128)(2,1)S(1)} all-to-all(bf16[32,2,8,128]{3,2,1,0:T(8,128)(2,1)S(1)} %bitcast.69), channel_id=1, replica_groups=mesh['ep'=32,'tp_0'=4,'tp_1'=4] {'ep'}, dimensions={0} | all-to-all | bytes 262144 | tf_op jit(solution)/shard_map/all_to_all | solution.py:81
  59.2 0.5 broadcast_in_dim.2
  59.7 0.0 copy-start.1
  59.7 29.9 %all_to_all.21 = bf16[16,32,2,8,128]{4,3,1,2,0:T(8,128)(2,1)S(1)} all-to-all(bf16[16,32,2,8,128]{4,3,1,2,0:T(8,128)(2,1)S(1)} %broadcast_in_dim.2), channel_id=1, replica_groups=mesh['ep'=32,'tp_0'=4,'tp_1'=4] {'tp_0','tp_1'}, dimensions={0} | all-to-all | bytes 4194304 | tf_op jit(solution)/shard_map/all_to_all | solution.py:25
  89.6 0.0 copy-done.1
  89.6 0.7 fusion.10
  90.3 0.0 copy-done
  90.3 3.9 %fusion.6 = bf16[32,2,8,16,128]{4,2,3,0,1:T(8,128)(2,1)} fusion(bf16[2,128,2048]{2,1,0:T(8,128)(2,1)S(1)} %copy-done, bf16[2,2048,128]{2,1,0:T(8,128)(2,1)} %param.12, f32[32,2,8,128]{3,2,0,1:T(8,128)S(1)} %fusion.10, bf16[16,32,2,8,128]{4,3,1,2,0:T(8,128)(2,1)S(1)} %all_to_all.21), kind=kOutput, calls=%fused_computation.8 | convolution fusion | flops 538509312 | bytes 6553600 | tf_op jit(solution)/shard_map/secf,efd->secd/dot_general | solution.py:86
  94.2 2.2 %copy.89 = bf16[32,2,8,16,128]{4,2,0,1,3:T(8,128)(2,1)S(1)} copy(bf16[32,2,8,16,128]{4,2,3,0,1:T(8,128)(2,1)} %fusion.6) | data formatting | bytes 4194304 | tf_op jit(solution)/shard_map/reshape | solution.py:41
  96.4 30.1 %all_to_all.22 = bf16[16,32,2,8,128]{4,3,1,2,0:T(8,128)(2,1)S(1)} all-to-all(bf16[16,32,2,8,128]{4,3,1,2,0:T(8,128)(2,1)S(1)} %bitcast.68), channel_id=1, replica_groups=mesh['ep'=32,'tp_0'=4,'tp_1'=4] {'tp_0','tp_1'}, dimensions={0} | all-to-all | bytes 4194304 | tf_op jit(solution)/shard_map/all_to_all | solution.py:47
  126.5 0.3 reduce_sum.52
  126.8 22.0 %all_to_all.23 = bf16[32,2,8,128]{3,2,1,0:T(8,128)(2,1)S(1)} all-to-all(bf16[32,2,8,128]{3,2,1,0:T(8,128)(2,1)S(1)} %copy.59), channel_id=1, replica_groups=mesh['ep'=32,'tp_0'=4,'tp_1'=4] {'ep'}, dimensions={0} | all-to-all | bytes 262144 | tf_op jit(solution)/shard_map/all_to_all | solution.py:88
  148.8 0.8 convolution_convert_fusion.2
  (4 shorter events, 0.0 us)
Async XLA Ops:
  0.0 90.3 %copy-start = (bf16[2,128,2048]{2,1,0:T(8,128)(2,1)S(1)}, bf16[2,128,2048]{2,1,0:T(8,128)(2,1)}, u32[]{:S(2)}) copy-start(bf16[2,128,2048]{2,1,0:T(8,128)(2,1)} %param.13) | copy-start | bytes 3145732
  59.7 29.9 %copy-start.1 = (bf16[2,2048,128]{2,1,0:T(8,128)(2,1)S(1)}, bf16[2,2048,128]{2,1,0:T(8,128)(2,1)}, u32[]{:S(2)}) copy-start(bf16[2,2048,128]{2,1,0:T(8,128)(2,1)} %param.11) | copy-start | bytes 3145732
where the time goes:
time: 150 us
  blocking collectives  136 us (91%)
  matrix products  6.35 us (4%)
  local copies, waits for them, and re-layouts  4.48 us (3%)
  other arithmetic  3.12 us (2%)
    all_to_all x1, blocking collectives, per_device(): lax.all_to_all(outgoing, 'ep', split_axis=0, concat_axis=0, tiled=True)  35.6 us
    all_to_all x1, blocking collectives, summed_on_arrival(): lax.all_to_all(pieces, axis, split_axis=0, concat_axis=0, tiled=True)  30.1 us
    all_to_all x1, blocking collectives, sent_to_all(): return lax.all_to_all(copies, axis, split_axis=0, concat_axis=0, tiled=True)  29.9 us
    all_to_all x1, blocking collectives, per_device(): lax.all_to_all(summed, 'ep', split_axis=0, concat_axis=0, tiled=True)  22 us
    psum x2, blocking collectives, one_axis_at_a_time(): return functools.reduce(lax.psum, axes, array)  18 us
    dot_general x1, matrix products, per_device(): jnp.einsum('secf,efd->secd', hidden, w_down, preferred_element_type=jnp.f...  3.92 us

commit v1 on v0

v1 whole, which is shorter than its diff:
```python
import jax
import jax.numpy as jnp
from jax import lax
from jax.sharding import PartitionSpec as P

D = 2048
CAP = 8

norm_eps = 1e-06
clamp_limit = 7.0
swish_alpha = 1.702


def activate(pre_gate, pre_up):
    clamped = jnp.minimum(pre_gate, clamp_limit)
    upper = jnp.clip(pre_up, -clamp_limit, clamp_limit)
    return (clamped * jax.nn.sigmoid(swish_alpha * clamped) * (upper + 1.0)).astype(jnp.bfloat16)


def per_device(tokens, routing, gate_weights, norm_gain, w_gate, w_up, w_down):
    ep_size = lax.axis_size("ep")
    exp_here = w_gate.shape[0]
    expert_count = exp_here * ep_size
    tok_rows = tokens.shape[0]
    top_count = routing.shape[1]
    col_width = tokens.shape[1]
    chosen = routing.reshape(-1)
    onehot = (chosen[:, None] == jnp.arange(expert_count, dtype=jnp.int32)[None, :]).astype(
        jnp.int32
    )
    slot_rank = jnp.sum(jnp.cumsum(onehot, axis=0) * onehot, axis=1) - 1
    slot_index = (chosen * CAP + slot_rank).reshape(tok_rows, top_count)
    slot_ids = jnp.arange(expert_count * CAP, dtype=jnp.int32)
    matches = slot_ids[:, None, None] == slot_index[None, :, :]
    placing = jnp.sum(matches.astype(jnp.float32), axis=2).astype(jnp.bfloat16)
    outgoing = jnp.dot(placing, tokens, preferred_element_type=jnp.float32).astype(jnp.bfloat16)
    outgoing = outgoing.reshape(ep_size, exp_here, CAP, col_width)
    received = lax.all_to_all(outgoing, "ep", split_axis=0, concat_axis=0, tiled=True)
    received = jnp.transpose(received, (1, 0, 2, 3)).reshape(exp_here, ep_size * CAP, col_width)
    raw = lax.all_gather(received, "tp", axis=2, tiled=True)
    wide = raw.astype(jnp.float32)
    ssq = jnp.sum(wide * wide, axis=2, keepdims=True)
    rows = (wide * lax.rsqrt(ssq / D + norm_eps) * norm_gain).astype(jnp.bfloat16)
    gate_part = jnp.einsum("erd,edf->erf", rows, w_gate, preferred_element_type=jnp.float32)
    up_part = jnp.einsum("erd,edf->erf", rows, w_up, preferred_element_type=jnp.float32)
    hidden = activate(gate_part, up_part)
    partial_value = jnp.einsum("erf,efd->erd", hidden, w_down, preferred_element_type=jnp.float32)
    summed = lax.psum_scatter(
        partial_value.astype(jnp.bfloat16), "tp", scatter_dimension=2, tiled=True
    )
    summed = jnp.transpose(summed.reshape(exp_here, ep_size, CAP, col_width), (1, 0, 2, 3))
    returned = lax.all_to_all(summed, "ep", split_axis=0, concat_axis=0, tiled=True)
    returned = returned.reshape(expert_count * CAP, col_width).astype(jnp.float32)
    combine = jnp.sum(matches.astype(jnp.float32) * gate_weights[None, :, :], axis=2)
    mixed = jnp.dot(combine.T, returned, precision=lax.Precision.HIGHEST)
    return mixed.astype(jnp.bfloat16)


def solution(mesh):
    placed = (
        P("ep", "tp"),
        P("ep", None),
        P("ep", None),
        P(),
        P("ep", None, "tp"),
        P("ep", None, "tp"),
        P("ep", "tp", None),
    )
    return jax.shard_map(
        per_device, mesh=mesh, in_specs=placed, out_specs=P("ep", "tp"), check_vma=False
    )
```

time: 150 us -> 241 us (1.61)
  waiting for transfers between devices: 0 us -> 143 us
  blocking collectives: 136 us -> 62.7 us
  between operations: 0.11 us -> 13.5 us
  local copies, waits for them, and re-layouts: 4.48 us -> 9.54 us
    unnamed x0 -> x3, waiting for transfers between devices: none -> 89.9 us
    all_to_all x2 -> x0, blocking collectives: 59.9 us -> none  [the longest x1 30.1 us: summed_on_arrival(): lax.all_to_all(pieces, axis, split_axis=0, concat_axis=0, tiled=True)]
    all_gather x0 -> x1, waiting for transfers between devices: none -> 53.2 us  [per_device(): raw = lax.all_gather(received, 'tp', axis=2, tiled=True)]
    psum x2 -> x0, blocking collectives: 18 us -> none  [one_axis_at_a_time(): return functools.reduce(lax.psum, axes, array)]
    all_to_all x1, blocking collectives: 22 us -> 30.3 us  [per_device(): lax.all_to_all(summed, 'ep', split_axis=0, concat_axis=0, tiled=True)]
    unnamed x5 -> x11, local copies, waits for them, and re-layouts: 0.78 us -> 8.58 us
    all_to_all x1, blocking collectives: 35.6 us -> 32.4 us  [per_device(): lax.all_to_all(outgoing, 'ep', split_axis=0, concat_axis=0, tiled=True)]
  transfers between devices with their start and end apart: 0 -> 2, of which waited for: 0 -> 2; matrix products, arithmetic and copies ran while one was open for 0% -> 0% of each run, Pallas kernels for 0% -> 0%
where the time goes in v1:
time: 241 us
  waiting for transfers between devices  143 us (59%)
  blocking collectives  62.7 us (26%)
  between operations  13.5 us (6%)
  local copies, waits for them, and re-layouts  9.54 us (4%)
  matrix products  7.72 us (3%)
  other arithmetic  4.16 us (2%)
    unnamed x3, waiting for transfers between devices  89.9 us
    all_gather x1, waiting for transfers between devices, per_device(): raw = lax.all_gather(received, 'tp', axis=2, tiled=True)  53.2 us
    all_to_all x1, blocking collectives, per_device(): lax.all_to_all(outgoing, 'ep', split_axis=0, concat_axis=0, tiled=True)  32.4 us
    all_to_all x1, blocking collectives, per_device(): lax.all_to_all(summed, 'ep', split_axis=0, concat_axis=0, tiled=True)  30.3 us
    unnamed x11, local copies, waits for them, and re-layouts  8.58 us
  transfers between devices with their start and end apart: 2, of which 2 were waited for; matrix products, arithmetic and copies ran while one was open for 0% of the time, Pallas kernels for 0%

profile of v1, /device:TPU:1, one launch (start us, length us, event | category | flops | bytes accessed | tf_op | source)
XLA Modules:
  0.0 240.7 jit_solution(11151847588226632373)
XLA Ops:
  6.5 0.0 copy-start
  6.5 0.0 copy-start.2
  6.5 0.0 all-gather.2.cloned.1.call-start
  6.5 0.9 copy.42
  7.4 0.1 eq.29
  7.5 0.1 fusion.34
  7.6 0.2 reduce_window_sum.11
  7.8 0.2 select_reduce_fusion.1
  8.0 0.1 sub.7
  8.1 0.1 copy.43
  8.2 0.7 multiply_add_fusion
  8.8 0.8 convert_reduce_fusion
  9.7 0.9 convolution_convert_fusion.1
  10.6 32.4 %all_to_all.10 = bf16[32,2,8,128]{3,2,1,0:T(8,128)(2,1)S(1)} all-to-all(bf16[32,2,8,128]{3,2,1,0:T(8,128)(2,1)S(1)} %bitcast.24), channel_id=1, replica_groups=mesh['ep'=32,'tp'=16] {'ep'}, dimensions={0} | all-to-all | bytes 262144 | tf_op jit(solution)/shard_map/all_to_all | solution.py:38
  43.0 0.7 copy_bitcast_fusion
  43.6 0.0 all-gather.2.cloned.1.call-update
  43.6 0.0 reduce-scatter.4.cloned.1.call-start
  43.7 53.2 %all-gather.2.cloned.1.call-done = bf16[2,256,2048]{2,1,0:T(8,128)(2,1)} async-done(((bf16[2,256,128]{2,1,0:T(8,128)(2,1)}), bf16[2,256,2048]{2,1,0:T(8,128)(2,1)}) %all-gather.2.cloned.1.call-update) | async-done | bytes 2097168 | tf_op jit(solution)/shard_map/all_gather | solution.py:40
  96.9 2.2 fusion
  99.1 0.0 copy-done.2
  99.1 0.0 copy-done.1
  99.1 2.0 fusion.7
  101.2 0.0 copy-done
  101.2 4.0 %convolution_convert_fusion = bf16[2,256,2048]{2,1,0:T(8,128)(2,1)} fusion(bf16[2,128,2048]{2,1,0:T(8,128)(2,1)S(1)} %copy-done, bf16[2,2048,128]{2,1,0:T(8,128)(2,1)} %param.12, bf16[2,256,2048]{2,1,0:T(8,128)(2,1)S(1)} %copy-done.1, f32[2048]{0:T(1024)S(1)} %copy-done.2, f32[2,256]{1,0:T(2,128)S(1)} %add_rsqrt_fusion, f32[2,256,128]{2,1,0:T(8,128)S(1)} %fusion.7), kind=kOutput, calls=%fused_computation.5 | convolution fusion | flops 542703616 | bytes 6563840 | tf_op jit(solution)/shard_map/erf,efd->erd/dot_general | solution.py:47
  105.2 4.8 %copy.46 = bf16[2,256,2048]{1,0,2:T(2,128)(2,1)S(1)} copy(bf16[2,256,2048]{2,1,0:T(8,128)(2,1)} %convolution_convert_fusion) | data formatting | bytes 4194304
  110.0 1.8 copy.48
  111.8 0.0 reduce-scatter.4.cloned.1.call-update
  111.8 89.9 %reduce-scatter.4.cloned.1.call-done = bf16[128,512]{1,0:T(8,128)(2,1)} async-done(((bf16[2048,512]{1,0:T(8,128)(2,1)}), bf16[128,512]{1,0:T(8,128)(2,1)}) %reduce-scatter.4.cloned.1.call-update) | async-done | bytes 131088
  201.7 0.9 reshape.38
  202.6 0.1 copy.47
  202.8 30.3 %all_to_all.11 = bf16[32,2,8,128]{3,2,1,0:T(8,128)(2,1)S(1)} all-to-all(bf16[32,2,8,128]{3,2,1,0:T(8,128)(2,1)S(1)} %copy.45), channel_id=1, replica_groups=mesh['ep'=32,'tp'=16] {'ep'}, dimensions={0} | all-to-all | bytes 262144 | tf_op jit(solution)/shard_map/all_to_all | solution.py:52
  233.1 0.8 convolution_convert_fusion.2
  (4 shorter events, 0.0 us)
Async XLA Ops:
  6.5 94.6 %copy-start = (bf16[2,128,2048]{2,1,0:T(8,128)(2,1)S(1)}, bf16[2,128,2048]{2,1,0:T(8,128)(2,1)}, u32[]{:S(2)}) copy-start(bf16[2,128,2048]{2,1,0:T(8,128)(2,1)} %param.13) | copy-start | bytes 3145732
  6.5 92.6 %copy-start.2 = (f32[2048]{0:T(1024)S(1)}, f32[2048]{0:T(1024)}, u32[]{:S(2)}) copy-start(f32[2048]{0:T(1024)} %param.10) | copy-start | bytes 24580
  6.5 90.3 %all-gather.2.cloned.1.call-start = ((), (), s32[]{:S(2)}) async-start(), calls=%async_computation.3 | async-start | bytes 2228224 | tf_op jit(solution)/shard_map/all_gather | solution.py:40
  43.6 158.0 %reduce-scatter.4.cloned.1.call-start = ((), (), s32[]{:S(2)}) async-start(), calls=%async_computation.4 | async-start | bytes 2228224
  96.9 2.2 copy-start.1
Sparse Core Ops, SparseCore 0:
  43.8 53.0 all-gather.1
  112.0 89.6 reduce-scatter.3

commit v2 on v1

v2 whole, which is shorter than its diff:
```python
import functools

import jax
import jax.numpy as jnp
from jax import lax
from jax.experimental import pallas as pl
from jax.experimental.pallas import tpu as pltpu
from jax.sharding import PartitionSpec as P

D = 2048
CAP = 8
NX = 4
NY = 4
NZ = 16
EXP_DEV = 2
LANES = 128
NC = 4
ORDER = (0, 1, -1, 2, -2, 3, -3, 4, -4, 5, -5, 6, -6, 7, -7, 8)
PER = NZ // NC
ROWS = PER * 2 * CAP
HALF = ROWS // 2

norm_eps = 1e-06
clamp_limit = 7.0
swish_alpha = 1.702
MESH = pl.DeviceIdType.MESH


def activate(pre_gate, pre_up):
    clamped = jnp.minimum(pre_gate, clamp_limit)
    upper = jnp.clip(pre_up, -clamp_limit, clamp_limit)
    return (clamped * jax.nn.sigmoid(swish_alpha * clamped) * (upper + 1.0)).astype(jnp.bfloat16)


def kernel(
    tok, rout, gw, gain, wg, wu, wd, out,
    outgoing, gath, part, rb1, rb2, quart, rb3, rb4, final, ret, wgu, wdn, comb,
    wsem, zs, zr, rs, rr, hs, hr,
):
    ep = lax.axis_index("ep")
    tp = lax.axis_index("tp")
    z, core = ep // 2, lax.rem(ep, 2)
    y, x = tp // NX, lax.rem(tp, NX)

    def ring(value, step, size):
        return lax.rem(value + step + size, size)

    def ep_at(dz, other):
        return ring(z, dz, NZ) * 2 + (lax.rem(core + other, 2))

    def beside(axis, step):
        if axis == "x":
            return {"tp": y * NX + ring(x, step, NX)}
        return {"tp": ring(y, step, NY) * NX + x}

    weights = [
        pltpu.make_async_copy(wg, wgu.at[:, :, pl.ds(0, LANES)], wsem.at[0]),
        pltpu.make_async_copy(wu, wgu.at[:, :, pl.ds(LANES, LANES)], wsem.at[1]),
        pltpu.make_async_copy(wd, wdn, wsem.at[2]),
    ]
    for copy in weights:
        copy.start()

    barrier = pltpu.get_barrier_semaphore()
    peers = [{"ep": ep_at(d, o)} for d in ORDER for o in range(2) if (d, o) != (0, 0)]
    peers += [beside(a, s) for a in ("x", "y") for s in (1, -1)]
    for peer in peers:
        pl.semaphore_signal(barrier, inc=1, device_id=peer, device_id_type=MESH)

    chosen = rout[...]
    lanes = lax.broadcasted_iota(jnp.int32, (32, 64), 1)
    hot = [jnp.where(chosen[:, k : k + 1] == lanes, 1.0, 0.0) for k in range(4)]
    named = hot[0] + hot[1] + hot[2] + hot[3]
    lower = jnp.where(
        lax.broadcasted_iota(jnp.int32, (32, 32), 0) > lax.broadcasted_iota(jnp.int32, (32, 32), 1),
        1.0, 0.0,
    )
    before = jnp.dot(
        lower.astype(jnp.bfloat16), named.astype(jnp.bfloat16), preferred_element_type=jnp.float32
    )
    slots = lax.broadcasted_iota(jnp.int32, (32, 512), 1)
    place = jnp.zeros((32, 512), jnp.float32)
    mix = jnp.zeros((32, 512), jnp.float32)
    for k in range(4):
        rank = jnp.sum(before * hot[k], axis=1, keepdims=True).astype(jnp.int32)
        match = (chosen[:, k : k + 1] * CAP + rank) == slots
        place = place + jnp.where(match, 1.0, 0.0)
        mix = mix + jnp.where(match, gw[:, k : k + 1], 0.0)
    comb[...] = mix
    outgoing[...] = lax.dot_general(
        place.astype(jnp.bfloat16), tok[...], (((0,), (0,)), ((), ())),
        preferred_element_type=jnp.float32,
    ).astype(jnp.bfloat16).reshape(32, EXP_DEV, CAP, LANES)

    pl.semaphore_wait(barrier, len(peers))

    sends = []

    def send(src, dst, ssem, rsem, device):
        copy = pltpu.make_async_remote_copy(
            src_ref=src, dst_ref=dst, send_sem=ssem, recv_sem=rsem, device_id=device,
            device_id_type=MESH,
        )
        copy.start()
        sends.append(copy)
        return copy

    place_of = {}
    for i, d in enumerate(ORDER):
        place_of[d % NZ] = (i // PER, i % PER)

    zcopies = {}
    for i, d in enumerate(ORDER):
        for o in range(2):
            c, k = place_of[(-d) % NZ]
            target = ep_at(d, o)
            where = 2 * k + o
            if (d, o) == (0, 0):
                own = outgoing[target]
                for e in range(EXP_DEV):
                    gath[c, y, x, e, where] = own[e]
                continue
            zcopies[(c, where)] = send(
                outgoing.at[target], gath.at[c, y, x, :, where],
                zs.at[c * 2 * PER + where], zr.at[c * 2 * PER + where], {"ep": target},
            )

    live = {}
    first, second = ("x", "y"), ("y", "x")

    def pos(axis):
        return x if axis == "x" else y

    def hop(name, c, h, axis, views):
        stage = ("a1", "a2", "a3", "a4", "r1", "r2", "r3", "r4").index(name)
        made = []
        for j, step in enumerate((1, -1)):
            src, dst = views[j]
            idx = ((stage * NC + c) * 2 + h) * 2 + j
            made.append(send(src, dst, rs.at[idx], rr.at[idx], beside(axis, step)))
        live[(name, c, h)] = made

    def landed(name, c, h):
        for copy in live[(name, c, h)]:
            copy.wait_recv()

    def block(c, h, i, j, lo=0, n=ROWS // CAP):
        return gath.at[c, i, j, h, pl.ds(lo, n)]

    def line(ref, c, h, axis, at, lo=0, n=ROWS // CAP):
        if axis == "y":
            return ref.at[c, at, :, h, pl.ds(lo, n)]
        return ref.at[c, :, at, h, pl.ds(lo, n)]

    K2 = HALF // CAP

    def s0(c):
        for key, copy in zcopies.items():
            if key[0] == c:
                copy.wait_recv()
        for h in range(2):
            view = block(c, h, y, x)
            hop("a1", c, h, first[h], [(view, view)] * 2)

    def s1(c):
        for h in range(2):
            landed("a1", c, h)
            a = first[h]
            back, ahead = ring(pos(a), -1, 4), ring(pos(a), 1, 4)
            if a == "x":
                v0, v1 = block(c, h, y, back, 0, K2), block(c, h, y, ahead, K2, K2)
            else:
                v0, v1 = block(c, h, back, x, 0, K2), block(c, h, ahead, x, K2, K2)
            hop("a2", c, h, a, [(v0, v0), (v1, v1)])

    def s2(c):
        for h in range(2):
            landed("a2", c, h)
            a = second[h]
            view = line(gath, c, h, a, pos(a))
            hop("a3", c, h, a, [(view, view)] * 2)

    def s3(c):
        for h in range(2):
            landed("a3", c, h)
            a = second[h]
            v0 = line(gath, c, h, a, ring(pos(a), -1, 4), 0, K2)
            v1 = line(gath, c, h, a, ring(pos(a), 1, 4), K2, K2)
            hop("a4", c, h, a, [(v0, v0), (v1, v1)])

    def s4(c):
        for h in range(2):
            landed("a4", c, h)
            if c == 0 and h == 0:
                for copy in weights:
                    copy.wait()
            raw = jnp.concatenate(
                [gath[c, i, j, h].reshape(ROWS, LANES) for i in range(NY) for j in range(NX)],
                axis=1,
            )
            wide = raw.astype(jnp.float32)
            ssq = jnp.sum(wide * wide, axis=1, keepdims=True)
            rows = (wide * lax.rsqrt(ssq / D + norm_eps) * gain[...]).astype(jnp.bfloat16)
            both = jnp.dot(rows, wgu[h], preferred_element_type=jnp.float32)
            hidden = activate(both[:, :LANES], both[:, LANES:])
            value = jnp.dot(hidden, wdn[h], preferred_element_type=jnp.float32).astype(jnp.bfloat16)
            for i in range(NY):
                for j in range(NX):
                    at = (i * NX + j) * LANES
                    part[c, i, j, h] = value[:, at : at + LANES].reshape(ROWS // CAP, CAP, LANES)
            a = second[h]
            far = ring(pos(a), 2, 4)
            hop("r1", c, h, a, [
                (line(part, c, h, a, far, 0, K2), rb1.at[c, h, 0]),
                (line(part, c, h, a, far, K2, K2), rb1.at[c, h, 1]),
            ])

    def add_into(ref_view, other):
        ref_view[...] = (
            ref_view[...].astype(jnp.float32) + other[...].astype(jnp.float32)
        ).astype(jnp.bfloat16)

    def s5(c):
        for h in range(2):
            landed("r1", c, h)
            a = second[h]
            ahead, back = ring(pos(a), 1, 4), ring(pos(a), -1, 4)
            add_into(line(part, c, h, a, ahead, 0, K2), rb1.at[c, h, 0])
            add_into(line(part, c, h, a, back, K2, K2), rb1.at[c, h, 1])
            hop("r2", c, h, a, [
                (line(part, c, h, a, ahead), rb2.at[c, h, 0]),
                (line(part, c, h, a, back), rb2.at[c, h, 1]),
            ])

    def s6(c):
        for h in range(2):
            landed("r2", c, h)
            a, b = second[h], first[h]
            total = line(part, c, h, a, pos(a))[...].astype(jnp.float32)
            total = total + rb2[c, h, 0].astype(jnp.float32) + rb2[c, h, 1].astype(jnp.float32)
            quart[c, h] = total.astype(jnp.bfloat16)
            far = ring(pos(b), 2, 4)
            hop("r3", c, h, b, [
                (quart.at[c, h, far, pl.ds(0, K2)], rb3.at[c, h, 0]),
                (quart.at[c, h, far, pl.ds(K2, K2)], rb3.at[c, h, 1]),
            ])

    def s7(c):
        for h in range(2):
            landed("r3", c, h)
            b = first[h]
            ahead, back = ring(pos(b), 1, 4), ring(pos(b), -1, 4)
            add_into(quart.at[c, h, ahead, pl.ds(0, K2)], rb3.at[c, h, 0])
            add_into(quart.at[c, h, back, pl.ds(K2, K2)], rb3.at[c, h, 1])
            hop("r4", c, h, b, [
                (quart.at[c, h, ahead], rb4.at[c, h, 0]),
                (quart.at[c, h, back], rb4.at[c, h, 1]),
            ])

    homes = []

    def s8(c):
        for h in range(2):
            landed("r4", c, h)
            b = first[h]
            total = quart[c, h, pos(b)].astype(jnp.float32)
            total = total + rb4[c, h, 0].astype(jnp.float32) + rb4[c, h, 1].astype(jnp.float32)
            final[c, h] = total.astype(jnp.bfloat16)
        for k in range(PER):
            d = ORDER[c * PER + k]
            for o in range(2):
                where = 2 * k + o
                if (d, o) == (0, 0):
                    for e in range(EXP_DEV):
                        ret[ep, e] = final[c, e, where]
                    continue
                i = (c * PER + k) * 2 + o
                homes.append(
                    send(
                        final.at[c, :, where], ret.at[ep],
                        hs.at[i], hr.at[i], {"ep": ep_at(d, o)},
                    )
                )

    stages = (s0, s1, s2, s3, s4, s5, s6, s7, s8)
    for t in range(len(stages) + NC - 1):
        for c in range(NC):
            if 0 <= t - c < len(stages):
                stages[t - c](c)

    for copy in homes:
        copy.wait_recv()
    mixed = jnp.dot(
        comb[...], ret[...].reshape(512, LANES).astype(jnp.float32),
        preferred_element_type=jnp.float32, precision=lax.Precision.HIGHEST,
    )
    out[...] = mixed.astype(jnp.bfloat16)
    for copy in sends:
        copy.wait_send()


def per_device(tokens, routing, gate_weights, norm_gain, w_gate, w_up, w_down):
    vmem = pl.BlockSpec(memory_space=pltpu.VMEM)
    hbm = pl.BlockSpec(memory_space=pl.ANY)
    tiles = ROWS // CAP
    bf = jnp.bfloat16
    hops = 8 * NC * 2 * 2
    return pl.pallas_call(
        kernel,
        out_shape=jax.ShapeDtypeStruct((32, LANES), bf),
        in_specs=[vmem, vmem, vmem, vmem, hbm, hbm, hbm],
        out_specs=vmem,
        scratch_shapes=[
            pltpu.VMEM((32, EXP_DEV, CAP, LANES), bf),
            pltpu.VMEM((NC, NY, NX, EXP_DEV, tiles, CAP, LANES), bf),
            pltpu.VMEM((NC, NY, NX, EXP_DEV, tiles, CAP, LANES), bf),
            pltpu.VMEM((NC, 2, 2, 4, tiles // 2, CAP, LANES), bf),
            pltpu.VMEM((NC, 2, 2, 4, tiles, CAP, LANES), bf),
            pltpu.VMEM((NC, 2, 4, tiles, CAP, LANES), bf),
            pltpu.VMEM((NC, 2, 2, tiles // 2, CAP, LANES), bf),
            pltpu.VMEM((NC, 2, 2, tiles, CAP, LANES), bf),
            pltpu.VMEM((NC, 2, tiles, CAP, LANES), bf),
            pltpu.VMEM((32, EXP_DEV, CAP, LANES), bf),
            pltpu.VMEM((EXP_DEV, D, 2 * LANES), bf),
            pltpu.VMEM((EXP_DEV, LANES, D), bf),
            pltpu.VMEM((32, 512), jnp.float32),
            pltpu.SemaphoreType.DMA((3,)),
            pltpu.SemaphoreType.DMA((32,)),
            pltpu.SemaphoreType.DMA((32,)),
            pltpu.SemaphoreType.DMA((hops,)),
            pltpu.SemaphoreType.DMA((hops,)),
            pltpu.SemaphoreType.DMA((32,)),
            pltpu.SemaphoreType.DMA((32,)),
        ],
        compiler_params=pltpu.CompilerParams(
            collective_id=0, has_side_effects=True, vmem_limit_bytes=48 * 1024 * 1024
        ),
        name="moe_step",
    )(tokens, routing, gate_weights, norm_gain.reshape(1, D), w_gate, w_up, w_down)


def solution(mesh):
    placed = (
        P("ep", "tp"),
        P("ep", None),
        P("ep", None),
        P(),
        P("ep", None, "tp"),
        P("ep", None, "tp"),
        P("ep", "tp", None),
    )
    return jax.shard_map(
        per_device, mesh=mesh, in_specs=placed, out_specs=P("ep", "tp"), check_vma=False
    )
```

time: 241 us -> 84.1 us (0.35)
  waiting for transfers between devices: 143 us -> 0 us
  Pallas kernels: 0 us -> 78 us
  blocking collectives: 62.7 us -> 0 us
  between operations: 13.5 us -> 0.02 us
  matrix products: 7.72 us -> 0 us
  other arithmetic: 4.16 us -> 0 us
  local copies, waits for them, and re-layouts: 9.54 us -> 5.76 us
    unnamed x3 -> x0, waiting for transfers between devices: 89.9 us -> none
    pallas_call x0 -> x1, Pallas kernels: none -> 78 us  [per_device(): pl.pallas_call(kernel, out_shape=jax.ShapeDtypeStruct((32, LANES), bf), i...]
    all_to_all x2 -> x0, blocking collectives: 62.7 us -> none  [the longest x1 32.4 us: per_device(): lax.all_to_all(outgoing, 'ep', split_axis=0, concat_axis=0, tiled=True)]
    all_gather x1 -> x0, waiting for transfers between devices: 53.2 us -> none  [per_device(): raw = lax.all_gather(received, 'tp', axis=2, tiled=True)]
    dot_general x4 -> x0, matrix products: 7.72 us -> none  [the longest x1 3.99 us: per_device(): jnp.einsum('erf,efd->erd', hidden, w_down, preferred_element_type=jnp.flo...]
    reduce_sum x3 -> x0, other arithmetic: 3.19 us -> none  [the longest x1 2.22 us: per_device(): ssq = jnp.sum(wide * wide, axis=2, keepdims=True)]
    unnamed x11 -> x15, local copies, waits for them, and re-layouts: 8.58 us -> 5.76 us
  transfers between devices with their start and end apart: 2 -> 0, of which waited for: 2 -> 0; matrix products, arithmetic and copies ran while one was open for 0% -> 0% of each run, Pallas kernels for 0% -> 0%
where the time goes in v2:
time: 84.1 us; the launch traced here: 83.8 us
  Pallas kernels  78 us (93%)
  local copies, waits for them, and re-layouts  5.76 us (7%)
    pallas_call x1, Pallas kernels, per_device(): pl.pallas_call(kernel, out_shape=jax.ShapeDtypeStruct((32, LANES), bf), i...  78 us
    unnamed x15, local copies, waits for them, and re-layouts  5.76 us

profile of v2, /device:TPU:1, one launch (start us, length us, event | category | flops | bytes accessed | tf_op | source)
XLA Modules:
  0.0 83.8 jit_solution(8877829967718566556)
XLA Ops:
  0.0 0.0 copy-start.5
  0.0 0.8 copy.8.rout
  0.8 0.0 copy-done.5
  0.8 0.0 copy-start.3
  0.8 0.0 copy-start.4
  0.8 0.1 copy.9.gw
  0.9 0.6 copy-done.3
  1.5 0.0 copy-done.4
  1.5 0.0 copy-start
  1.5 1.2 %copy-done = bf16[2,2048,128]{2,1,0:T(8,128)(2,1)S(1)} copy-done((bf16[2,2048,128]{2,1,0:T(8,128)(2,1)S(1)}, bf16[2,2048,128]{2,1,0:T(8,128)(2,1)}, u32[]{:S(2)}) %copy-start) | copy-done | bytes 1048600
  2.7 0.0 copy-start.1
  2.7 1.2 %copy-done.1 = bf16[2,2048,128]{2,1,0:T(8,128)(2,1)S(1)} copy-done((bf16[2,2048,128]{2,1,0:T(8,128)(2,1)S(1)}, bf16[2,2048,128]{2,1,0:T(8,128)(2,1)}, u32[]{:S(2)}) %copy-start.1) | copy-done | bytes 1048600
  3.9 0.0 copy-start.2
  3.9 1.2 %copy-done.2 = bf16[2,128,2048]{2,1,0:T(8,128)(2,1)S(1)} copy-done((bf16[2,128,2048]{2,1,0:T(8,128)(2,1)S(1)}, bf16[2,128,2048]{2,1,0:T(8,128)(2,1)}, u32[]{:S(2)}) %copy-start.2) | copy-done | bytes 1048600
  5.2 78.0 %moe_step.1 = bf16[32,128]{1,0:T(8,128)(2,1)S(1)} custom-call(bf16[32,128]{1,0:T(8,128)(2,1)S(1)} %copy-done.3, s32[32,4]{1,0:T(8,128)S(1)} %copy.8.rout, f32[32,4]{1,0:T(8,128)S(1)} %copy.9.gw, f32[1,2048]{1,0:T(1,128)S(1)} %bitcast.1, bf16[2,2048,128]{2,1,0:T(8,128)(2,1)S(1)} %copy-done, bf16[2,2048,128]{2,1,0:T(8,128)(2,1)S(1)} %copy-done.1, ...), custom_call_target="tpu_custom_call" | custom-call | tf_op jit(solution)/shard_map/moe_step/pallas_call | solution.py:308
  83.2 0.6 copy.11
Async XLA Ops:
  0.0 0.8 copy-start.5
  0.8 0.7 copy-start.3
  0.8 0.7 copy-start.4
  1.5 1.2 %copy-start = (bf16[2,2048,128]{2,1,0:T(8,128)(2,1)S(1)}, bf16[2,2048,128]{2,1,0:T(8,128)(2,1)}, u32[]{:S(2)}) copy-start(bf16[2,2048,128]{2,1,0:T(8,128)(2,1)} %wg.1) | copy-start | bytes 3145732
  2.7 1.2 %copy-start.1 = (bf16[2,2048,128]{2,1,0:T(8,128)(2,1)S(1)}, bf16[2,2048,128]{2,1,0:T(8,128)(2,1)}, u32[]{:S(2)}) copy-start(bf16[2,2048,128]{2,1,0:T(8,128)(2,1)} %wu.1) | copy-start | bytes 3145732
  3.9 1.2 %copy-start.2 = (bf16[2,128,2048]{2,1,0:T(8,128)(2,1)S(1)}, bf16[2,128,2048]{2,1,0:T(8,128)(2,1)}, u32[]{:S(2)}) copy-start(bf16[2,128,2048]{2,1,0:T(8,128)(2,1)} %wd.1) | copy-start | bytes 3145732

commit v3 on v1

v3 whole, which is shorter than its diff:
```python
import functools

import jax
import jax.numpy as jnp
from jax import lax
from jax.experimental import pallas as pl
from jax.experimental.pallas import tpu as pltpu
from jax.sharding import PartitionSpec as P

D = 2048
CAP = 8
NX = 4
NY = 4
NZ = 16
EXP_DEV = 2
LANES = 128
NC = 2
ORDER = (8, -7, 7, -6, 6, -5, 5, -4, 4, -3, 3, -2, 2, -1, 1, 0)
PER = NZ // NC
ROWS = PER * 2 * CAP
HALF = ROWS // 2

PLAN = (
    ("a1", 0, 0),
    ("a1", 0, 1),
    ("a3", 0, 0),
    ("a3", 0, 1),
    ("a1", 1, 0),
    ("a1", 1, 1),
    ("a4", 0, 0),
    ("a4", 0, 1),
    ("a3", 1, 1),
    ("a3", 1, 0),
    ("r1", 0, 0),
    ("r1", 0, 1),
    ("a4", 1, 1),
    ("a4", 1, 0),
    ("r2", 0, 0),
    ("r2", 0, 1),
    ("r1", 1, 0),
    ("r1", 1, 1),
    ("r3", 0, 0),
    ("r3", 0, 1),
    ("r2", 1, 0),
    ("r2", 1, 1),
    ("fin", 0, 0),
    ("fin", 0, 1),
    ("r3", 1, 0),
    ("r3", 1, 1),
    ("fin", 1, 0),
    ("fin", 1, 1),
)
WEIGHTS_AT = (0, 0)
GOES = ((0, 1), (1, 1))

norm_eps = 1e-06
clamp_limit = 7.0
swish_alpha = 1.702
MESH = pl.DeviceIdType.MESH


def activate(pre_gate, pre_up):
    clamped = jnp.minimum(pre_gate, clamp_limit)
    upper = jnp.clip(pre_up, -clamp_limit, clamp_limit)
    return (clamped * jax.nn.sigmoid(swish_alpha * clamped) * (upper + 1.0)).astype(jnp.bfloat16)


def kernel(
    tok_in, rout_in, gw_in, gain_in, wg, wu, wd, out,
    tok, rout, gw, gain, outgoing, gath, part, rb1, rb2, quart, rb4, final, ret, wgu, wdn, comb,
    wsem, zs, zr, rs, rr, hs, hr,
):
    ep = lax.axis_index("ep")
    tp = lax.axis_index("tp")
    z, core = ep // 2, lax.rem(ep, 2)
    y, x = tp // NX, lax.rem(tp, NX)

    def ring(value, step, size):
        return lax.rem(value + step + size, size)

    def ep_at(dz, other):
        return ring(z, dz, NZ) * 2 + (lax.rem(core + other, 2))

    def beside(axis, step):
        if axis == "x":
            return {"tp": y * NX + ring(x, step, NX)}
        return {"tp": ring(y, step, NY) * NX + x}

    weights = [
        pltpu.make_async_copy(wg, wgu.at[:, :, pl.ds(0, LANES)], wsem.at[0]),
        pltpu.make_async_copy(wu, wgu.at[:, :, pl.ds(LANES, LANES)], wsem.at[1]),
        pltpu.make_async_copy(wd, wdn, wsem.at[2]),
    ]
    loads = [
        pltpu.make_async_copy(src, dst, wsem.at[3 + i])
        for i, (src, dst) in enumerate(
            ((rout_in, rout), (tok_in, tok), (gw_in, gw), (gain_in, gain))
        )
    ]
    for copy in loads:
        copy.start()

    barrier = pltpu.get_barrier_semaphore()
    peers = [{"ep": ep_at(d, o)} for d in ORDER for o in range(2) if (d, o) != (0, 0)]
    peers += [beside(a, s) for a in ("x", "y") for s in (1, -1, 2)]
    for peer in peers:
        pl.semaphore_signal(barrier, inc=1, device_id=peer, device_id_type=MESH)

    for copy in loads[:3]:
        copy.wait()
    for copy in weights:
        copy.start()
    chosen = rout[...]
    names = lax.broadcasted_iota(jnp.int32, (64, 32), 0)
    hot = [jnp.where(chosen[k : k + 1, :] == names, 1.0, 0.0) for k in range(4)]
    named = hot[0] + hot[1] + hot[2] + hot[3]
    upper = jnp.where(
        lax.broadcasted_iota(jnp.int32, (32, 32), 0) < lax.broadcasted_iota(jnp.int32, (32, 32), 1),
        1.0, 0.0,
    )
    before = jnp.dot(
        named.astype(jnp.bfloat16), upper.astype(jnp.bfloat16), preferred_element_type=jnp.float32
    )
    slots = lax.broadcasted_iota(jnp.int32, (512, 32), 0)
    place = jnp.zeros((512, 32), jnp.float32)
    mix = jnp.zeros((512, 32), jnp.float32)
    for k in range(4):
        rank = jnp.sum(before * hot[k], axis=0, keepdims=True).astype(jnp.int32)
        match = (chosen[k : k + 1, :] * CAP + rank) == slots
        place = place + jnp.where(match, 1.0, 0.0)
        mix = mix + jnp.where(match, gw[k : k + 1, :], 0.0)
    comb[...] = mix
    outgoing[...] = jnp.dot(
        place.astype(jnp.bfloat16), tok[...], preferred_element_type=jnp.float32
    ).astype(jnp.bfloat16).reshape(32, EXP_DEV, CAP, LANES)

    pl.semaphore_wait(barrier, len(peers))

    sends = []

    def send(src, dst, ssem, rsem, device):
        copy = pltpu.make_async_remote_copy(
            src_ref=src, dst_ref=dst, send_sem=ssem, recv_sem=rsem, device_id=device,
            device_id_type=MESH,
        )
        copy.start()
        sends.append(copy)
        return copy

    mine, where = ep // (2 * PER), lax.rem(ep, 2 * PER)
    for d in ORDER:
        for o in range(2):
            target = ep_at(d, o)
            if (d, o) == (0, 0):
                own = outgoing[target]
                for e in range(EXP_DEV):
                    gath[mine, y, x, e, where] = own[e]
                continue
            send(
                outgoing.at[target], gath.at[mine, y, x, :, where],
                zs.at[(d % NZ) * 2 + o], zr.at[ep], {"ep": target},
            )

    live = {}
    first, second = ("x", "y"), ("y", "x")

    def pos(axis):
        return x if axis == "x" else y

    def hop(name, c, h, axis, views):
        stage = ("a1", "a3", "a4", "r1", "r2", "r3").index(name)
        made = []
        for j, step in enumerate((1, -1, 2)[: len(views)]):
            src, dst = views[j]
            idx = ((stage * NC + c) * 2 + h) * 3 + j
            made.append(send(src, dst, rs.at[idx], rr.at[idx], beside(axis, step)))
        live[(name, c, h)] = made

    def landed(name, c, h):
        for copy in live[(name, c, h)]:
            copy.wait_recv()

    def block(c, h, i, j, lo=0, n=ROWS // CAP):
        return gath.at[c, i, j, h, pl.ds(lo, n)]

    def line(ref, c, h, axis, at, lo=0, n=ROWS // CAP):
        if axis == "y":
            return ref.at[c, at, :, h, pl.ds(lo, n)]
        return ref.at[c, :, at, h, pl.ds(lo, n)]

    K2 = HALF // CAP

    def select(c):
        for i in range(2 * PER):
            source = c * 2 * PER + i

            @pl.when(ep != source)
            def _(source=source, i=i):
                pltpu.make_async_remote_copy(
                    src_ref=outgoing.at[source], dst_ref=gath.at[c, y, x, :, i],
                    send_sem=zs.at[0], recv_sem=zr.at[source], device_id={"ep": source},
                    device_id_type=MESH,
                ).wait_recv()

    def a1(c, h):
        view = block(c, h, y, x)
        hop("a1", c, h, first[h], [(view, view)] * 3)

    def a3(c, h):
        landed("a1", c, h)
        a = second[h]
        view = line(gath, c, h, a, pos(a))
        hop("a3", c, h, a, [(view, view)] * 2)

    def a4(c, h):
        landed("a3", c, h)
        a = second[h]
        v0 = line(gath, c, h, a, ring(pos(a), -1, 4), 0, K2)
        v1 = line(gath, c, h, a, ring(pos(a), 1, 4), K2, K2)
        hop("a4", c, h, a, [(v0, v0), (v1, v1)])

    def r1(c, h):
        landed("a4", c, h)
        if (c, h) == WEIGHTS_AT:
            for copy in weights + loads[3:]:
                copy.wait()
        raw = jnp.concatenate(
            [gath[c, i, j, h].reshape(ROWS, LANES) for i in range(NY) for j in range(NX)],
            axis=1,
        )
        wide = raw.astype(jnp.float32)
        ssq = jnp.sum(wide * wide, axis=1, keepdims=True)
        rows = (wide * lax.rsqrt(ssq / D + norm_eps) * gain[...]).astype(jnp.bfloat16)
        both = jnp.dot(rows, wgu[h], preferred_element_type=jnp.float32)
        hidden = activate(both[:, :LANES], both[:, LANES:])
        value = jnp.dot(hidden, wdn[h], preferred_element_type=jnp.float32).astype(jnp.bfloat16)
        for i in range(NY):
            for j in range(NX):
                at = (i * NX + j) * LANES
                part[c, i, j, h] = value[:, at : at + LANES].reshape(ROWS // CAP, CAP, LANES)
        a = second[h]
        far = ring(pos(a), 2, 4)
        hop("r1", c, h, a, [
            (line(part, c, h, a, far, 0, K2), rb1.at[c, h, 0]),
            (line(part, c, h, a, far, K2, K2), rb1.at[c, h, 1]),
        ])

    def add_into(ref_view, other):
        ref_view[...] = (
            ref_view[...].astype(jnp.float32) + other[...].astype(jnp.float32)
        ).astype(jnp.bfloat16)

    def r2(c, h):
        landed("r1", c, h)
        a = second[h]
        ahead, back = ring(pos(a), 1, 4), ring(pos(a), -1, 4)
        add_into(line(part, c, h, a, ahead, 0, K2), rb1.at[c, h, 0])
        add_into(line(part, c, h, a, back, K2, K2), rb1.at[c, h, 1])
        hop("r2", c, h, a, [
            (line(part, c, h, a, ahead), rb2.at[c, h, 0]),
            (line(part, c, h, a, back), rb2.at[c, h, 1]),
        ])

    def r3(c, h):
        landed("r2", c, h)
        a, b = second[h], first[h]
        total = line(part, c, h, a, pos(a))[...].astype(jnp.float32)
        total = total + rb2[c, h, 0].astype(jnp.float32) + rb2[c, h, 1].astype(jnp.float32)
        quart[c, h] = total.astype(jnp.bfloat16)
        hop("r3", c, h, b, [
            (quart.at[c, h, ring(pos(b), step, 4)], rb4.at[c, h, j])
            for j, step in enumerate((1, -1, 2))
        ])

    def fin(c, h):
        landed("r3", c, h)
        total = quart[c, h, pos(first[h])].astype(jnp.float32)
        for j in range(3):
            total = total + rb4[c, h, j].astype(jnp.float32)
        final[c, h] = total.astype(jnp.bfloat16)
        if (c, h) in GOES:
            go_home(c)

    def home(c, i, target):
        return pltpu.make_async_remote_copy(
            src_ref=final.at[c, :, i], dst_ref=ret.at[ep],
            send_sem=hs.at[target], recv_sem=hr.at[ep], device_id={"ep": target},
            device_id_type=MESH,
        )

    def go_home(c):
        for i in range(2 * PER):
            target = c * 2 * PER + i

            @pl.when(ep == target)
            def _(target=target, i=i):
                for e in range(EXP_DEV):
                    ret[target, e] = final[c, e, i]

            @pl.when(ep != target)
            def _(target=target, i=i):
                home(c, i, target).start()

    stages = dict(a1=a1, a3=a3, a4=a4, r1=r1, r2=r2, r3=r3, fin=fin)
    done = set()
    for name, c, h in PLAN:
        if c not in done:
            done.add(c)
            select(c)
        stages[name](c, h)

    for source in range(32):

        @pl.when(ep != source)
        def _(source=source):
            copy = pltpu.make_async_remote_copy(
                src_ref=final.at[source // (2 * PER), :, source % (2 * PER)], dst_ref=ret.at[source],
                send_sem=hs.at[source], recv_sem=hr.at[source], device_id={"ep": source},
                device_id_type=MESH,
            )
            copy.wait_recv()
            copy.wait_send()

    mixed = lax.dot_general(
        comb[...], ret[...].reshape(512, LANES).astype(jnp.float32), (((0,), (0,)), ((), ())),
        preferred_element_type=jnp.float32, precision=lax.Precision.HIGHEST,
    )
    out[...] = mixed.astype(jnp.bfloat16)
    for copy in sends:
        copy.wait_send()


def per_device(tokens, routing, gate_weights, norm_gain, w_gate, w_up, w_down):
    vmem = pl.BlockSpec(memory_space=pltpu.VMEM)
    hbm = pl.BlockSpec(memory_space=pltpu.HBM)
    tiles = ROWS // CAP
    bf = jnp.bfloat16
    hops = 6 * NC * 2 * 3
    return pl.pallas_call(
        kernel,
        out_shape=jax.ShapeDtypeStruct((32, LANES), bf),
        in_specs=[hbm] * 7,
        out_specs=vmem,
        scratch_shapes=[
            pltpu.VMEM((32, LANES), bf),
            pltpu.VMEM((4, 32), jnp.int32),
            pltpu.VMEM((4, 32), jnp.float32),
            pltpu.VMEM((1, D), jnp.float32),
            pltpu.VMEM((32, EXP_DEV, CAP, LANES), bf),
            pltpu.VMEM((NC, NY, NX, EXP_DEV, tiles, CAP, LANES), bf),
            pltpu.VMEM((NC, NY, NX, EXP_DEV, tiles, CAP, LANES), bf),
            pltpu.VMEM((NC, 2, 2, 4, tiles // 2, CAP, LANES), bf),
            pltpu.VMEM((NC, 2, 2, 4, tiles, CAP, LANES), bf),
            pltpu.VMEM((NC, 2, 4, tiles, CAP, LANES), bf),
            pltpu.VMEM((NC, 2, 3, tiles, CAP, LANES), bf),
            pltpu.VMEM((NC, 2, tiles, CAP, LANES), bf),
            pltpu.VMEM((32, EXP_DEV, CAP, LANES), bf),
            pltpu.VMEM((EXP_DEV, D, 2 * LANES), bf),
            pltpu.VMEM((EXP_DEV, LANES, D), bf),
            pltpu.VMEM((512, 32), jnp.float32),
            pltpu.SemaphoreType.DMA((7,)),
            pltpu.SemaphoreType.DMA((32,)),
            pltpu.SemaphoreType.DMA((32,)),
            pltpu.SemaphoreType.DMA((hops,)),
            pltpu.SemaphoreType.DMA((hops,)),
            pltpu.SemaphoreType.DMA((32,)),
            pltpu.SemaphoreType.DMA((32,)),
        ],
        compiler_params=pltpu.CompilerParams(
            collective_id=0, has_side_effects=True, vmem_limit_bytes=67043328
        ),
        name="moe_step",
    )(tokens, routing.T, gate_weights.T, norm_gain.reshape(1, D), w_gate, w_up, w_down)


def solution(mesh):
    placed = (
        P("ep", "tp"),
        P("ep", None),
        P("ep", None),
        P(),
        P("ep", None, "tp"),
        P("ep", None, "tp"),
        P("ep", "tp", None),
    )
    return jax.shard_map(
        per_device, mesh=mesh, in_specs=placed, out_specs=P("ep", "tp"), check_vma=False
    )
```

time: 241 us -> 67.5 us (0.28)
  waiting for transfers between devices: 143 us -> 0 us
  Pallas kernels: 0 us -> 66 us
  blocking collectives: 62.7 us -> 0 us
  between operations: 13.5 us -> 0.01 us
  local copies, waits for them, and re-layouts: 9.54 us -> 1.3 us
  matrix products: 7.72 us -> 0 us
  other arithmetic: 4.16 us -> 0 us
    unnamed x3 -> x0, waiting for transfers between devices: 89.9 us -> none
    pallas_call x0 -> x1, Pallas kernels: none -> 66 us  [per_device(): pl.pallas_call(kernel, out_shape=jax.ShapeDtypeStruct((32, LANES), bf), i...]
    all_to_all x2 -> x0, blocking collectives: 62.7 us -> none  [the longest x1 32.4 us: per_device(): lax.all_to_all(outgoing, 'ep', split_axis=0, concat_axis=0, tiled=True)]
    all_gather x1 -> x0, waiting for transfers between devices: 53.2 us -> none  [per_device(): raw = lax.all_gather(received, 'tp', axis=2, tiled=True)]
    dot_general x4 -> x0, matrix products: 7.72 us -> none  [the longest x1 3.99 us: per_device(): jnp.einsum('erf,efd->erd', hidden, w_down, preferred_element_type=jnp.flo...]
    unnamed x11 -> x1, local copies, waits for them, and re-layouts: 8.58 us -> 1.3 us
    reduce_sum x3 -> x0, other arithmetic: 3.19 us -> none  [the longest x1 2.22 us: per_device(): ssq = jnp.sum(wide * wide, axis=2, keepdims=True)]
  transfers between devices with their start and end apart: 2 -> 0, of which waited for: 2 -> 0; matrix products, arithmetic and copies ran while one was open for 0% -> 0% of each run, Pallas kernels for 0% -> 0%
where the time goes in v3:
time: 67.5 us; the launch traced here: 67.3 us
  Pallas kernels  66 us (98%)
  local copies, waits for them, and re-layouts  1.3 us (2%)
    pallas_call x1, Pallas kernels, per_device(): pl.pallas_call(kernel, out_shape=jax.ShapeDtypeStruct((32, LANES), bf), i...  66 us

profile of v3, /device:TPU:1, one launch (start us, length us, event | category | flops | bytes accessed | tf_op | source)
XLA Modules:
  0.0 67.3 jit_solution(7805437202918155895)
XLA Ops:
  0.0 66.0 %moe_step.1 = bf16[32,128]{1,0:T(8,128)(2,1)} custom-call(bf16[32,128]{1,0:T(8,128)(2,1)} %tok_in.1, s32[4,32]{1,0:T(4,128)} %bitcast.4, f32[4,32]{1,0:T(4,128)} %bitcast.5, f32[1,2048]{1,0:T(1,128)} %bitcast.3, bf16[2,2048,128]{2,1,0:T(8,128)(2,1)} %wg.1, bf16[2,2048,128]{2,1,0:T(8,128)(2,1)} %wu.1, bf16[2,128,2048]{2,1,0:T(8,128)(2,1)} %wd.1), custom_call_target="tpu_custom_call" | custom-call | tf_op jit(solution)/shard_map/moe_step/pallas_call | solution.py:339
  66.0 1.3 %copy.9 = bf16[32,128]{1,0:T(8,128)(2,1)} copy(bf16[32,128]{1,0:T(8,128)(2,1)} %moe_step.1) | data formatting | bytes 16384

commit v4 on v3

--- a/solution.py
+++ b/solution.py
@@ -14,7 +14,7 @@
 NZ = 16
 EXP_DEV = 2
 LANES = 128
-NC = 2
+NC = 4
 ORDER = (8, -7, 7, -6, 6, -5, 5, -4, 4, -3, 3, -2, 2, -1, 1, 0)
 PER = NZ // NC
 ROWS = PER * 2 * CAP
@@ -23,35 +23,63 @@
 PLAN = (
     ("a1", 0, 0),
     ("a1", 0, 1),
+    ("a1", 1, 0),
+    ("a1", 1, 1),
     ("a3", 0, 0),
     ("a3", 0, 1),
-    ("a1", 1, 0),
-    ("a1", 1, 1),
+    ("a1", 2, 0),
+    ("a1", 2, 1),
+    ("a1", 3, 0),
+    ("a1", 3, 1),
+    ("a3", 1, 0),
+    ("a3", 1, 1),
     ("a4", 0, 0),
     ("a4", 0, 1),
-    ("a3", 1, 1),
-    ("a3", 1, 0),
+    ("a3", 2, 1),
+    ("a3", 2, 0),
+    ("a3", 3, 1),
+    ("a3", 3, 0),
+    ("a4", 1, 0),
+    ("a4", 1, 1),
     ("r1", 0, 0),
     ("r1", 0, 1),
-    ("a4", 1, 1),
-    ("a4", 1, 0),
+    ("a4", 2, 0),
+    ("a4", 2, 1),
+    ("a4", 3, 0),
+    ("a4", 3, 1),
+    ("r1", 1, 0),
     ("r2", 0, 0),
+    ("r1", 1, 1),
     ("r2", 0, 1),
-    ("r1", 1, 0),
-    ("r1", 1, 1),
+    ("r1", 2, 0),
+    ("r1", 2, 1),
+    ("r2", 1, 0),
+    ("r1", 3, 0),
+    ("r2", 1, 1),
     ("r3", 0, 0),
+    ("r1", 3, 1),
     ("r3", 0, 1),
-    ("r2", 1, 0),
-    ("r2", 1, 1),
+    ("r2", 2, 0),
+    ("r2", 2, 1),
+    ("r3", 1, 0),
+    ("r2", 3, 0),
+    ("r3", 1, 1),
+    ("fin", 0, 1),
     ("fin", 0, 0),
-    ("fin", 0, 1),
-    ("r3", 1, 0),
-    ("r3", 1, 1),
+    ("r2", 3, 1),
+    ("r3", 2, 0),
+    ("r3", 2, 1),
+    ("r3", 3, 0),
     ("fin", 1, 0),
     ("fin", 1, 1),
+    ("r3", 3, 1),
+    ("fin", 2, 0),
+    ("fin", 2, 1),
+    ("fin", 3, 0),
+    ("fin", 3, 1),
 )
 WEIGHTS_AT = (0, 0)
-GOES = ((0, 1), (1, 1))
+GOES = ((0, 0), (1, 1), (2, 1), (3, 1))
 
 norm_eps = 1e-06
 clamp_limit = 7.0
@@ -129,7 +157,11 @@
         match = (chosen[k : k + 1, :] * CAP + rank) == slots
         place = place + jnp.where(match, 1.0, 0.0)
         mix = mix + jnp.where(match, gw[k : k + 1, :], 0.0)
-    comb[...] = mix
+    mix = mix.T
+    for n in range(3):
+        term = mix.astype(jnp.bfloat16)
+        comb[pl.ds(32 * n, 32), :] = term
+        mix = mix - term.astype(jnp.float32)
     outgoing[...] = jnp.dot(
         place.astype(jnp.bfloat16), tok[...], preferred_element_type=jnp.float32
     ).astype(jnp.bfloat16).reshape(32, EXP_DEV, CAP, LANES)
@@ -309,6 +341,9 @@
             select(c)
         stages[name](c, h)
 
+    for copy in sends:
+        copy.wait_send()
+
     for source in range(32):
 
         @pl.when(ep != source)
@@ -321,13 +356,10 @@
             copy.wait_recv()
             copy.wait_send()
 
-    mixed = lax.dot_general(
-        comb[...], ret[...].reshape(512, LANES).astype(jnp.float32), (((0,), (0,)), ((), ())),
-        preferred_element_type=jnp.float32, precision=lax.Precision.HIGHEST,
+    terms = jnp.dot(
+        comb[...], ret[...].reshape(512, LANES), preferred_element_type=jnp.float32
     )
-    out[...] = mixed.astype(jnp.bfloat16)
-    for copy in sends:
-        copy.wait_send()
+    out[...] = (terms[:32] + terms[32:64] + terms[64:]).astype(jnp.bfloat16)
 
 
 def per_device(tokens, routing, gate_weights, norm_gain, w_gate, w_up, w_down):
@@ -357,7 +389,7 @@
             pltpu.VMEM((32, EXP_DEV, CAP, LANES), bf),
             pltpu.VMEM((EXP_DEV, D, 2 * LANES), bf),
             pltpu.VMEM((EXP_DEV, LANES, D), bf),
-            pltpu.VMEM((512, 32), jnp.float32),
+            pltpu.VMEM((96, 512), bf),
             pltpu.SemaphoreType.DMA((7,)),
             pltpu.SemaphoreType.DMA((32,)),
             pltpu.SemaphoreType.DMA((32,)),

time: 67.5 us -> 65.8 us (0.975)
  Pallas kernels: 66 us -> 64.3 us
    pallas_call x1, Pallas kernels: 66 us -> 64.3 us  [per_device(): pl.pallas_call(kernel, out_shape=jax.ShapeDtypeStruct((32, LANES), bf), i...]
where the time goes in v4:
time: 65.8 us; the launch traced here: 65.6 us
  Pallas kernels  64.3 us (98%)
  local copies, waits for them, and re-layouts  1.3 us (2%)
    pallas_call x1, Pallas kernels, per_device(): pl.pallas_call(kernel, out_shape=jax.ShapeDtypeStruct((32, LANES), bf), i...  64.3 us

profile of v4, /device:TPU:1, one launch (start us, length us, event | category | flops | bytes accessed | tf_op | source)
XLA Modules:
  0.0 65.6 jit_solution(16706954310051112344)
XLA Ops:
  0.0 64.3 %moe_step.1 = bf16[32,128]{1,0:T(8,128)(2,1)} custom-call(bf16[32,128]{1,0:T(8,128)(2,1)} %tok_in.1, s32[4,32]{1,0:T(4,128)} %bitcast.4, f32[4,32]{1,0:T(4,128)} %bitcast.5, f32[1,2048]{1,0:T(1,128)} %bitcast.3, bf16[2,2048,128]{2,1,0:T(8,128)(2,1)} %wg.1, bf16[2,2048,128]{2,1,0:T(8,128)(2,1)} %wu.1, bf16[2,128,2048]{2,1,0:T(8,128)(2,1)} %wd.1), custom_call_target="tpu_custom_call" | custom-call | tf_op jit(solution)/shard_map/moe_step/pallas_call | solution.py:371
  64.3 1.3 %copy.9 = bf16[32,128]{1,0:T(8,128)(2,1)} copy(bf16[32,128]{1,0:T(8,128)(2,1)} %moe_step.1) | data formatting | bytes 16384

commit v5 on v4

--- a/solution.py
+++ b/solution.py
@@ -202,7 +202,8 @@
     def hop(name, c, h, axis, views):
         stage = ("a1", "a3", "a4", "r1", "r2", "r3").index(name)
         made = []
-        for j, step in enumerate((1, -1, 2)[: len(views)]):
+        steps = ((0, 1), (1, -1)) if len(views) == 2 else ((2, 2), (0, 1), (1, -1))
+        for j, step in steps:
             src, dst = views[j]
             idx = ((stage * NC + c) * 2 + h) * 3 + j
             made.append(send(src, dst, rs.at[idx], rr.at[idx], beside(axis, step)))

time: 65.8 us -> 66.1 us (level)
  no operation moved by 1% of the time
where the time goes in v5:
time: 66.1 us; the launch traced here: 65.9 us
  Pallas kernels  64.6 us (98%)
  local copies, waits for them, and re-layouts  1.3 us (2%)
    pallas_call x1, Pallas kernels, per_device(): pl.pallas_call(kernel, out_shape=jax.ShapeDtypeStruct((32, LANES), bf), i...  64.6 us

profile of v5, /device:TPU:1, one launch (start us, length us, event | category | flops | bytes accessed | tf_op | source)
XLA Modules:
  0.0 65.9 jit_solution(18378860358007337547)
XLA Ops:
  0.0 64.6 %moe_step.1 = bf16[32,128]{1,0:T(8,128)(2,1)} custom-call(bf16[32,128]{1,0:T(8,128)(2,1)} %tok_in.1, s32[4,32]{1,0:T(4,128)} %bitcast.4, f32[4,32]{1,0:T(4,128)} %bitcast.5, f32[1,2048]{1,0:T(1,128)} %bitcast.3, bf16[2,2048,128]{2,1,0:T(8,128)(2,1)} %wg.1, bf16[2,2048,128]{2,1,0:T(8,128)(2,1)} %wu.1, bf16[2,128,2048]{2,1,0:T(8,128)(2,1)} %wd.1), custom_call_target="tpu_custom_call" | custom-call | tf_op jit(solution)/shard_map/moe_step/pallas_call | solution.py:372
  64.6 1.3 %copy.9 = bf16[32,128]{1,0:T(8,128)(2,1)} copy(bf16[32,128]{1,0:T(8,128)(2,1)} %moe_step.1) | data formatting | bytes 16384
